TPU v7x, 32 devices: a whole 2x2x4 slice. The times are simulated.
32 devices in a mesh: ep: 4 (over y, x), tp: 8 (over z, core).
Axes of the slice: x: 2, y: 2, z: 4, core: 2. Of those that a mesh axis runs over, the one named last changes fastest.
Arguments:
- hidden: bfloat16 [64, 2048], P('ep'), may hold values from -6 to 6
- attn_gain: float32 [2048], replicated, may hold values from 0.1 to 1.9
- query_weight: bfloat16 [2048, 1024], P(None, 'tp'), may hold values from -0.125 to 0.125
- rotary_weight: bfloat16 [2048, 512], P(None, 'tp'), may hold values from -0.125 to 0.125
- key_up: bfloat16 [16, 64, 512], P('tp'), may hold values from -0.75 to 0.75
- cache_latent: bfloat16 [64, 4096, 512], P(('ep', 'tp'))
- cache_rotary: bfloat16 [64, 32, 4096], P(('ep', 'tp')), may hold values from -6 to 6
- lengths: int32 [64], P(('ep', 'tp')), may hold values from 1 to 4096, as said below
- value_up: bfloat16 [16, 512, 64], P('tp'), may hold values from -0.25 to 0.25
- out_weight: bfloat16 [1024, 2048], P('tp'), may hold values from -0.1875 to 0.1875
- mixed_gain: float32 [2048], replicated, may hold values from 0.1 to 1.9
- moe_gain: float32 [2048], replicated, may hold values from 0.1 to 1.9
- expert_ids: int32 [64, 2], replicated, may hold values from 0 to 3, all different within a row; in each aligned block of 16 rows (0 to 15, 16 to 31, ...) at most 16 rows name the same one
- route_logits: float32 [64, 2], replicated, may hold values from -6 to 6
- gate_weight: bfloat16 [4, 2048, 7168], P('ep', None, 'tp'), may hold values from -0.125 to 0.125
- up_weight: bfloat16 [4, 2048, 7168], P('ep', None, 'tp'), may hold values from -0.125 to 0.125
- down_weight: bfloat16 [4, 7168, 2048], P('ep', 'tp'), may hold values from -0.0625 to 0.0625
- final_gain: float32 [2048], replicated, may hold values from 0.1 to 1.9
Outputs:
- layer_out: bfloat16 [64, 2048], P(('ep', 'tp'))
Inputs may be any that keep to these rules, and one draw needn't show every extreme that they name: `lengths`: some sequence has exactly 4096 filled positions. `expert_ids`: within each aligned block of 16 rows no expert is named more than 16 times, a bound that some block reaches.
All inputs are finite; a program needn't handle non-finite values.
Results may differ from a plain program's by a relative error of at most 0.023.
The roundings to bfloat16 on the way count: a program that leaves them out, or rounds other values in their place, can miss the bound.
Values may be sent and summed in bfloat16 or wider, within the bound.
A program may use at most 64 MiB of HBM per device.

v0:
```python
import jax
import jax.numpy as jnp
from jax import lax
from jax.sharding import PartitionSpec as P

EPSILON = 1e-06


def norm_rows(values, gain_vector):
    values = values.astype(jnp.float32)
    factor = lax.rsqrt(jnp.mean(values * values, axis=-1, keepdims=True) + EPSILON)
    return values * factor * gain_vector


def rotate(values, position):
    half_width = values.shape[-1] // 2
    inverse = 10000.0 ** (-jnp.arange(half_width, dtype=jnp.float32) / half_width)
    angles = position.astype(jnp.float32)[:, None, None] * inverse
    cosine = jnp.cos(angles)
    sine_part = jnp.sin(angles)
    first_half = values[..., :half_width]
    second = values[..., half_width:]
    return jnp.concatenate(
        [first_half * cosine - second * sine_part, second * cosine + first_half * sine_part],
        axis=-1,
    )


def slot_tables(group_ids, group_probs, experts, capacity):
    row_count, top_count = group_ids.shape
    flat_ids = group_ids.reshape(-1)
    onehot = (flat_ids[:, None] == jnp.arange(experts, dtype=jnp.int32)[None, :]).astype(jnp.int32)
    earlier = jnp.cumsum(onehot, axis=0) - onehot
    slot_index = jnp.sum(earlier * onehot, axis=1)
    target = flat_ids * capacity + slot_index
    source = jnp.arange(row_count * top_count, dtype=jnp.int32) // top_count
    slot_rows = jnp.full((experts * capacity,), row_count, jnp.int32).at[target].set(source)
    slot_gates = (
        jnp.zeros((experts * capacity,), jnp.float32).at[target].set(group_probs.reshape(-1))
    )
    return (slot_rows, slot_gates)


def expert_rows(picked, gate_weight, up_weight, down_weight):
    gate_part = jnp.einsum("jnd,jdf->jnf", picked, gate_weight, preferred_element_type=jnp.float32)
    up_part = jnp.einsum("jnd,jdf->jnf", picked, up_weight, preferred_element_type=jnp.float32)
    act = (jax.nn.silu(gate_part) * up_part).astype(jnp.bfloat16)
    return jnp.einsum("jnf,jfd->jnd", act, down_weight, preferred_element_type=jnp.float32)


def body(
    hidden,
    attn_gain,
    query_weight,
    rotary_weight,
    key_up,
    cache_latent,
    cache_rotary,
    lengths,
    value_up,
    out_weight,
    mixed_gain,
    moe_gain,
    expert_ids,
    route_logits,
    gate_weight,
    up_weight,
    down_weight,
    final_gain,
):
    group_rows, features = hidden.shape
    local_heads, nope_width, latent_width = key_up.shape
    rotary_width = rotary_weight.shape[1] // local_heads
    own_rows = cache_latent.shape[0]
    groups = lax.axis_size("ep")
    own_start = lax.axis_index("tp") * own_rows
    normed_in = norm_rows(hidden, attn_gain).astype(jnp.bfloat16)
    query_nope = jnp.dot(normed_in, query_weight, preferred_element_type=jnp.float32).astype(
        jnp.bfloat16
    )
    query_nope = query_nope.reshape(group_rows, local_heads, nope_width)
    query_pe = jnp.dot(normed_in, rotary_weight, preferred_element_type=jnp.float32).astype(
        jnp.bfloat16
    )
    query_pe = query_pe.reshape(group_rows, local_heads, rotary_width)
    query_latent = jnp.einsum(
        "shn,hnc->shc", query_nope, key_up, preferred_element_type=jnp.float32
    ).astype(jnp.bfloat16)
    query_latent, query_pe = (
        lax.all_to_all(query_latent, "tp", split_axis=0, concat_axis=1, tiled=True),
        lax.all_to_all(query_pe, "tp", split_axis=0, concat_axis=1, tiled=True),
    )
    query_rot = rotate(query_pe.astype(jnp.float32), lengths - 1).astype(jnp.bfloat16)
    score_scale = (nope_width + rotary_width) ** (-0.5)
    scores = jnp.einsum(
        "bhc,bpc->bhp", query_latent, cache_latent, preferred_element_type=jnp.float32
    )
    scores = scores + jnp.einsum(
        "bhr,brp->bhp", query_rot, cache_rotary, preferred_element_type=jnp.float32
    )
    scores = scores * score_scale
    visible = (
        jnp.arange(cache_latent.shape[1], dtype=jnp.int32)[None, None, :] < lengths[:, None, None]
    )
    scores = jnp.where(visible, scores, -jnp.inf)
    highest = jnp.max(scores, axis=-1, keepdims=True)
    weights = jnp.exp(scores - highest)
    probs = (weights / jnp.sum(weights, axis=-1, keepdims=True)).astype(jnp.bfloat16)
    out_latent = jnp.einsum(
        "bhp,bpc->bhc", probs, cache_latent, preferred_element_type=jnp.float32
    ).astype(jnp.bfloat16)
    out_latent = lax.all_to_all(out_latent, "tp", split_axis=1, concat_axis=0, tiled=True)
    head_out = jnp.einsum(
        "shc,hcv->shv", out_latent, value_up, preferred_element_type=jnp.float32
    ).astype(jnp.bfloat16)
    head_terms = jnp.dot(
        head_out.reshape(group_rows, -1), out_weight, preferred_element_type=jnp.float32
    )
    attended = lax.psum(head_terms.astype(jnp.bfloat16), "tp")
    mixed_group = (hidden.astype(jnp.float32) + norm_rows(attended, mixed_gain)).astype(
        jnp.bfloat16
    )
    normed = norm_rows(mixed_group, moe_gain).astype(jnp.bfloat16)
    mixed_rows = lax.dynamic_slice_in_dim(mixed_group, own_start, own_rows, 0)
    local_experts = gate_weight.shape[0]
    experts_all = local_experts * groups
    top_count = expert_ids.shape[1]
    capacity = 2 * group_rows * top_count // experts_all
    gate_probs = jax.nn.softmax(route_logits, axis=-1)
    gathered = lax.all_gather(normed, "ep", axis=0, tiled=True)
    all_count = gathered.shape[0]

    def tables_for(group_ids, group_probs):
        return slot_tables(group_ids, group_probs, experts_all, capacity)

    slot_rows, slot_gates = jax.vmap(tables_for)(
        expert_ids.reshape(groups, group_rows, top_count),
        gate_probs.reshape(groups, group_rows, top_count),
    )
    offsets = jnp.arange(groups, dtype=jnp.int32)[:, None] * group_rows
    global_rows = jnp.where(slot_rows < group_rows, slot_rows + offsets, all_count)
    first_expert = lax.axis_index("ep") * local_experts
    my_rows = lax.dynamic_slice_in_dim(
        global_rows.reshape(groups, experts_all, capacity), first_expert, local_experts, 1
    )
    my_gates = lax.dynamic_slice_in_dim(
        slot_gates.reshape(groups, experts_all, capacity), first_expert, local_experts, 1
    )
    my_rows = my_rows.transpose(1, 0, 2).reshape(local_experts, groups * capacity)
    my_gates = my_gates.transpose(1, 0, 2).reshape(local_experts, groups * capacity)
    padded_all = jnp.concatenate([gathered, jnp.zeros((1, features), jnp.bfloat16)], axis=0)
    result = (
        expert_rows(padded_all[my_rows], gate_weight, up_weight, down_weight) * my_gates[..., None]
    )
    spread = (
        jnp.zeros((all_count + 1, features), jnp.float32)
        .at[my_rows.reshape(-1)]
        .add(result.reshape(-1, features))
    )
    routed = lax.psum_scatter(spread[:all_count], ("ep", "tp"), scatter_dimension=0, tiled=True)
    routed = routed.astype(jnp.bfloat16)
    return (mixed_rows.astype(jnp.float32) + norm_rows(routed, final_gain)).astype(jnp.bfloat16)


def solution(mesh):
    placed = (
        P("ep", None),
        P(),
        P(None, "tp"),
        P(None, "tp"),
        P("tp", None, None),
        P(("ep", "tp"), None, None),
        P(("ep", "tp"), None, None),
        P(("ep", "tp")),
        P("tp", None, None),
        P("tp", None),
        P(),
        P(),
        P(),
        P(),
        P("ep", None, "tp"),
        P("ep", None, "tp"),
        P("ep", "tp", None),
        P(),
    )
    return jax.shard_map(
        body, mesh=mesh, in_specs=placed, out_specs=P(("ep", "tp"), None), check_vma=False
    )
```

profile of v0, /device:TPU:0, one launch (start us, length us, event | category | flops | bytes accessed | tf_op | source)
XLA Modules:
  0.0 193.6 jit_solution(2101767761909809505)
XLA Ops:
  6.6 1.1 fusion.37
  7.6 1.2 convolution_convert_fusion.4
  8.9 0.7 reshape.273
  9.6 6.4 %all-to-all-start.1 = ((bf16[16,2,32]{2,1,0:T(2,128)(2,1)}), bf16[16,2,32]{2,1,0:T(2,128)(2,1)S(1)}, u32[]{:S(2)}, u32[]{:S(2)}) async-start(bf16[16,2,32]{2,1,0:T(2,128)(2,1)} %reshape.273), calls=%async_computation.1 | async-start | bytes 16384 | tf_op jit(solution)/shard_map/all_to_all | solution.py:91
  15.9 0.7 add_convert_fusion.1
  16.6 0.7 iota_compare_fusion.1
  17.3 0.8 copy.46
  18.1 0.7 broadcast_multiply_fusion
  18.8 0.1 eq.15
  18.9 0.1 fusion.42
  19.1 0.2 select_reduce_fusion
  19.3 0.1 copy.45
  19.4 0.1 mul.205
  19.6 0.1 reshape.301
  19.7 6.4 %scatter_fusion = s32[4,64]{1,0:T(4,128)S(1)} fusion(s32[4,64]{1,0:T(4,128)S(1)} %broadcast.223, s32[128]{0:T(128)S(1)} %reshape.299, s32[128]{0:T(128)S(1)} %reshape.301), kind=kCustom, calls=%fused_computation.2 | custom fusion | bytes 2560 | tf_op jit(solution)/shard_map/vmap()/scatter | solution.py:37
  26.1 0.1 reshape.275
  26.2 0.1 reshape_transpose.3
  26.4 0.2 convolution_convert_fusion.5
  26.7 0.1 reshape.272
  26.8 0.1 multiply_cosine_fusion
  26.9 0.1 fusion.20
  27.1 0.6 copy.39
  27.7 0.1 copy.48
  27.8 0.1 reshape.307
  28.0 6.4 %scatter_fusion.1 = f32[4,64]{1,0:T(4,128)S(1)} fusion(f32[4,64]{1,0:T(4,128)S(1)} %broadcast_in_dim.26, s32[128]{0:T(128)S(1)} %reshape.299, f32[128]{0:T(128)S(1)} %reshape.307), kind=kCustom, calls=%fused_computation.3 | custom fusion | bytes 2560 | tf_op jit(solution)/shard_map/vmap()/scatter | solution.py:39
  34.5 5.1 %all-to-all-start = ((bf16[16,2,512]{2,1,0:T(2,128)(2,1)}), bf16[16,2,512]{2,1,0:T(2,128)(2,1)S(1)}, u32[]{:S(2)}, u32[]{:S(2)}) async-start(bf16[16,2,512]{2,1,0:T(2,128)(2,1)} %copy.39), calls=%async_computation | async-start | bytes 65536 | tf_op jit(solution)/shard_map/all_to_all | solution.py:90
  39.6 5.7 %all-to-all-done = bf16[16,2,512]{2,1,0:T(2,128)(2,1)S(1)} async-done(((bf16[16,2,512]{2,1,0:T(2,128)(2,1)}), bf16[16,2,512]{2,1,0:T(2,128)(2,1)S(1)}, u32[]{:S(2)}, u32[]{:S(2)}) %all-to-all-start) | async-done | bytes 32800 | tf_op jit(solution)/shard_map/all_to_all | solution.py:90
  45.3 5.7 %fusion.66 = f32[2,16,4096]{2,1,0:T(8,128)S(1)} fusion(bf16[2,16,512]{2,1,0:T(8,128)(2,1)S(1)} %all_to_all.36, bf16[2,4096,512]{2,1,0:T(8,128)(2,1)} %param.23), kind=kOutput, calls=%fused_computation.111 | convolution fusion | flops 134217728 | bytes 8945664 | tf_op jit(solution)/shard_map/bhc,bpc->bhp/dot_general | solution.py:95
  51.0 0.3 fusion.3
  51.3 0.3 fusion.65
  51.6 4.7 %convolution_convert_fusion.1 = bf16[2,16,512]{2,1,0:T(8,128)(2,1)S(1)} fusion(bf16[2,4096,512]{2,1,0:T(8,128)(2,1)} %param.23, f32[2,16]{1,0:T(2,128)S(1)} %fusion.65, f32[2,16,4096]{2,1,0:T(8,128)S(1)} %fusion.3), kind=kOutput, calls=%fused_computation.20 | convolution fusion | flops 134631456 | bytes 8945792 | tf_op jit(solution)/shard_map/bhp,bpc->bhc/dot_general | solution.py:109
  56.3 0.6 copy.42
  57.0 3.3 %all-to-all-start.2 = ((bf16[2,16,512]{2,0,1:T(2,128)(2,1)}), bf16[2,16,512]{2,0,1:T(2,128)(2,1)S(1)}, u32[]{:S(2)}, u32[]{:S(2)}) async-start(bf16[2,16,512]{2,0,1:T(2,128)(2,1)} %copy.42), calls=%async_computation.2 | async-start | bytes 65536 | tf_op jit(solution)/shard_map/all_to_all | solution.py:112
  60.4 5.6 %all-to-all-done.2 = bf16[2,16,512]{2,0,1:T(2,128)(2,1)S(1)} async-done(((bf16[2,16,512]{2,0,1:T(2,128)(2,1)}), bf16[2,16,512]{2,0,1:T(2,128)(2,1)S(1)}, u32[]{:S(2)}, u32[]{:S(2)}) %all-to-all-start.2) | async-done | bytes 32800 | tf_op jit(solution)/shard_map/all_to_all | solution.py:112
  66.1 0.1 fusion.21
  66.2 0.1 reshape.274
  66.3 0.8 convolution_convert_fusion
  67.3 53.0 %all-reduce.5.cloned.1.call-done = bf16[16,2048]{1,0:T(8,128)(2,1)} async-done(((bf16[16,2048]{1,0:T(8,128)(2,1)}), bf16[16,2048]{1,0:T(8,128)(2,1)}) %all-reduce.5.cloned.1.call-update) | async-done | bytes 65552 | tf_op jit(solution)/shard_map/psum | solution.py:119
  120.3 1.0 fusion.32
  121.3 1.1 fusion.34
  122.4 9.3 %all_gather.3 = bf16[64,2048]{1,0:T(8,128)(2,1)S(1)} all-gather(bf16[16,2048]{1,0:T(8,128)(2,1)S(1)} %fusion.36), channel_id=1, replica_groups=mesh['ep'=4,'tp'=8] {'ep'}, dimensions={0}, use_global_device_ids=true | all-gather | bytes 327680 | tf_op jit(solution)/shard_map/all_gather | solution.py:130
  131.7 0.7 gather_fusion
  132.5 2.7 %fusion.9 = f32[64,896]{1,0:T(8,128)S(1)} fusion(bf16[64,2048]{1,0:T(8,128)(2,1)S(1)} %gather_fusion, bf16[1,2048,896]{2,1,0:T(8,128)(2,1)} %param.32), kind=kOutput, calls=%fused_computation.14 | convolution fusion | flops 234881024 | bytes 4161536 | tf_op jit(solution)/shard_map/jnd,jdf->jnf/dot_general | solution.py:45
  135.2 4.7 %fusion.11 = f32[64,2048]{1,0:T(8,128)S(1)} fusion(bf16[1,896,2048]{2,1,0:T(8,128)(2,1)} %param.34, bf16[64,2048]{1,0:T(8,128)(2,1)S(1)} %gather_fusion, bf16[1,2048,896]{2,1,0:T(8,128)(2,1)} %param.33, f32[64]{0:T(128)S(1)} %mul.215, f32[64,896]{1,0:T(8,128)S(1)} %fusion.9), kind=kOutput, calls=%fused_computation.16 | convolution fusion | flops 470237184 | bytes 8356096 | tf_op jit(solution)/shard_map/jnf,jfd->jnd/dot_general | solution.py:48
  140.0 1.5 scatter_custom_fusion
  141.5 44.3 %all-reduce.6 = bf16[64,2048]{1,0:T(8,128)(2,1)S(1)} all-reduce(f32[64,2048]{1,0:T(8,128)S(1)} %slice.20), channel_id=2, replica_groups=mesh['ep'=4,'tp'=8] {'ep','tp'}, use_global_device_ids=true, to_apply=%region_13.14.clone | all-reduce | flops 131072 | bytes 786432
  185.9 0.1 fusion.43
  186.0 0.7 fusion.46
  (60 shorter events, 1.1 us)
Async XLA Ops:
  6.5 44.5 %copy-start = (bf16[2,32,4096]{2,1,0:T(8,128)(2,1)S(1)}, bf16[2,32,4096]{2,1,0:T(8,128)(2,1)}, u32[]{:S(2)}) copy-start(bf16[2,32,4096]{2,1,0:T(8,128)(2,1)} %param.24) | copy-start | bytes 1572868
  6.5 19.9 %copy-start.1 = (bf16[16,2048]{1,0:T(8,128)(2,1)S(1)}, bf16[16,2048]{1,0:T(8,128)(2,1)}, u32[]{:S(2)}) copy-start(bf16[16,2048]{1,0:T(8,128)(2,1)} %param.18) | copy-start | bytes 196612
  6.5 19.9 %copy-start.7 = (f32[2048]{0:T(1024)S(1)}, f32[2048]{0:T(1024)}, u32[]{:S(2)}) copy-start(f32[2048]{0:T(1024)} %param.19) | copy-start | bytes 24580
  6.5 19.9 %copy-start.3 = (bf16[2048,128]{1,0:T(8,128)(2,1)S(1)}, bf16[2048,128]{1,0:T(8,128)(2,1)}, u32[]{:S(2)}) copy-start(bf16[2048,128]{1,0:T(8,128)(2,1)} %param.20) | copy-start | bytes 1572868
  6.5 20.2 %copy-start.6 = (f32[64,2]{0,1:T(2,128)S(1)}, f32[64,2]{0,1:T(2,128)}, u32[]{:S(2)}) copy-start(f32[64,2]{0,1:T(2,128)} %param.31) | copy-start | bytes 1540
  6.5 20.4 %copy-start.4 = (bf16[2,64,512]{2,1,0:T(8,128)(2,1)S(1)}, bf16[2,64,512]{2,1,0:T(8,128)(2,1)}, u32[]{:S(2)}) copy-start(bf16[2,64,512]{2,1,0:T(8,128)(2,1)} %param.22) | copy-start | bytes 393220
  9.6 24.9 %all-to-all-start.1 = ((bf16[16,2,32]{2,1,0:T(2,128)(2,1)}), bf16[16,2,32]{2,1,0:T(2,128)(2,1)S(1)}, u32[]{:S(2)}, u32[]{:S(2)}) async-start(bf16[16,2,32]{2,1,0:T(2,128)(2,1)} %reshape.273), calls=%async_computation.1 | async-start | bytes 16384 | tf_op jit(solution)/shard_map/all_to_all | solution.py:91
  34.5 10.8 %all-to-all-start = ((bf16[16,2,512]{2,1,0:T(2,128)(2,1)}), bf16[16,2,512]{2,1,0:T(2,128)(2,1)S(1)}, u32[]{:S(2)}, u32[]{:S(2)}) async-start(bf16[16,2,512]{2,1,0:T(2,128)(2,1)} %copy.39), calls=%async_computation | async-start | bytes 65536 | tf_op jit(solution)/shard_map/all_to_all | solution.py:90
  51.6 14.5 %copy-start.5 = (bf16[2,512,64]{1,2,0:T(8,128)(2,1)S(1)}, bf16[2,512,64]{1,2,0:T(8,128)(2,1)}, u32[]{:S(2)}) copy-start(bf16[2,512,64]{1,2,0:T(8,128)(2,1)} %param.26) | copy-start | bytes 393220
  51.6 14.7 %copy-start.2 = (bf16[128,2048]{1,0:T(8,128)(2,1)S(1)}, bf16[128,2048]{1,0:T(8,128)(2,1)}, u32[]{:S(2)}) copy-start(bf16[128,2048]{1,0:T(8,128)(2,1)} %param.27) | copy-start | bytes 1572868
  51.6 69.7 %copy-start.8 = (f32[2048]{0:T(1024)S(1)}, f32[2048]{0:T(1024)}, u32[]{:S(2)}) copy-start(f32[2048]{0:T(1024)} %param.28) | copy-start | bytes 24580
  51.6 70.7 %copy-start.9 = (f32[2048]{0:T(1024)S(1)}, f32[2048]{0:T(1024)}, u32[]{:S(2)}) copy-start(f32[2048]{0:T(1024)} %param.29) | copy-start | bytes 24580
  57.0 9.0 %all-to-all-start.2 = ((bf16[2,16,512]{2,0,1:T(2,128)(2,1)}), bf16[2,16,512]{2,0,1:T(2,128)(2,1)S(1)}, u32[]{:S(2)}, u32[]{:S(2)}) async-start(bf16[2,16,512]{2,0,1:T(2,128)(2,1)} %copy.42), calls=%async_computation.2 | async-start | bytes 65536 | tf_op jit(solution)/shard_map/all_to_all | solution.py:112
  60.3 60.0 %all-reduce.5.cloned.1.call-start = ((), (), s32[]{:S(2)}) async-start(), calls=%async_computation.3 | async-start | bytes 131072 | tf_op jit(solution)/shard_map/psum | solution.py:119
  135.2 50.8 %copy-start.10 = (f32[2048]{0:T(1024)S(1)}, f32[2048]{0:T(1024)}, u32[]{:S(2)}) copy-start(f32[2048]{0:T(1024)} %param.35) | copy-start | bytes 24580
Sparse Core Ops, SparseCore 0:
  67.3 52.9 all-reduce.4
where the time goes:
time: 194 us
  waiting for transfers between devices  64.3 us (33%)
  blocking collectives  53.6 us (28%)
  matrix products  20.7 us (11%)
  local copies, waits for them, and re-layouts  17.8 us (9%)
  starting transfers between devices  14.8 us (8%)
  between operations  13.7 us (7%)
  other arithmetic  8.61 us (4%)
    psum x1, waiting for transfers between devices, body(): attended = lax.psum(head_terms.astype(jnp.bfloat16), 'tp')  53 us
    unnamed x1, blocking collectives  44.3 us
    all_gather x1, blocking collectives, body(): gathered = lax.all_gather(normed, 'ep', axis=0, tiled=True)  9.29 us
    scatter x2, local copies, waits for them, and re-layouts, slot_tables(): jnp.full((experts * capacity,), row_count, jnp.int32).at[target].set(source)  6.48 us
    scatter x1, local copies, waits for them, and re-layouts, slot_tables(): jnp.zeros((experts * capacity,), jnp.float32).at[target]  6.4 us
    all_to_all x1, starting transfers between devices, body(): lax.all_to_all(query_pe, 'tp', split_axis=0, concat_axis=1, tiled=True)  6.35 us
    dot_general x1, matrix products, body(): jnp.einsum('bhc,bpc->bhp', query_latent, cache_latent, preferred_element_...  5.66 us
    all_to_all x1, waiting for transfers between devices, body(): lax.all_to_all(query_latent, 'tp', split_axis=0, concat_axis=1, tiled=True)  5.65 us
  transfers between devices with their start and end apart: 4, of which 3 were waited for; matrix products, arithmetic and copies ran while one was open for 10% of the time, Pallas kernels for 0%

commit v1 on v0

--- a/solution.py
+++ b/solution.py
@@ -4,6 +4,7 @@
 from jax.sharding import PartitionSpec as P
 
 EPSILON = 1e-06
+row_treat = lambda panel, mesh_ax: lax.all_gather(panel, mesh_ax).sum(axis=0)
 
 
 def norm_rows(values, gain_vector):
@@ -116,7 +117,7 @@
     head_terms = jnp.dot(
         head_out.reshape(group_rows, -1), out_weight, preferred_element_type=jnp.float32
     )
-    attended = lax.psum(head_terms.astype(jnp.bfloat16), "tp")
+    attended = row_treat(head_terms.astype(jnp.bfloat16), "tp")
     mixed_group = (hidden.astype(jnp.float32) + norm_rows(attended, mixed_gain)).astype(
         jnp.bfloat16
     )

time: 194 us -> 140 us (0.72)
  waiting for transfers between devices: 64.3 us -> 11.3 us
  blocking collectives: 53.6 us -> 67.9 us
  between operations: 13.7 us -> 0.3 us
    psum x1 -> x0, waiting for transfers between devices: 53 us -> none  [body(): attended = lax.psum(head_terms.astype(jnp.bfloat16), 'tp')]
    all_gather x0 -> x1, blocking collectives: none -> 15.1 us  [lax.all_gather(panel, mesh_ax).sum(axis=0)]
  transfers between devices with their start and end apart: 4 -> 3, of which waited for: 3 -> 2; matrix products, arithmetic and copies ran while one was open for 10% -> 13% of each run, Pallas kernels for 0% -> 0%
where the time goes in v1:
time: 140 us; the launch traced here: 139 us
  blocking collectives  67.9 us (49%)
  matrix products  20 us (14%)
  local copies, waits for them, and re-layouts  17.8 us (13%)
  starting transfers between devices  14.8 us (11%)
  waiting for transfers between devices  11.3 us (8%)
  other arithmetic  7 us (5%)
    unnamed x1, blocking collectives  43.9 us
    all_gather x1, blocking collectives, lax.all_gather(panel, mesh_ax).sum(axis=0)  15.1 us
    all_gather x1, blocking collectives, body(): gathered = lax.all_gather(normed, 'ep', axis=0, tiled=True)  8.99 us
    scatter x2, local copies, waits for them, and re-layouts, slot_tables(): jnp.full((experts * capacity,), row_count, jnp.int32).at[target].set(source)  6.48 us
    scatter x1, local copies, waits for them, and re-layouts, slot_tables(): jnp.zeros((experts * capacity,), jnp.float32).at[target]  6.4 us
    all_to_all x1, starting transfers between devices, body(): lax.all_to_all(query_pe, 'tp', split_axis=0, concat_axis=1, tiled=True)  6.36 us
    dot_general x1, matrix products, body(): jnp.einsum('bhc,bpc->bhp', query_latent, cache_latent, preferred_element_...  5.66 us
    all_to_all x1, waiting for transfers between devices, body(): lax.all_to_all(out_latent, 'tp', split_axis=1, concat_axis=0, tiled=True)  5.66 us
  transfers between devices with their start and end apart: 3, of which 2 were waited for; matrix products, arithmetic and copies ran while one was open for 13% of the time, Pallas kernels for 0%

profile of v1, /device:TPU:0, one launch (start us, length us, event | category | flops | bytes accessed | tf_op | source)
XLA Modules:
  0.0 139.2 jit_solution(10829412127954395125)
XLA Ops:
  0.0 1.1 fusion.37
  1.1 1.2 convolution_convert_fusion.4
  2.3 0.7 reshape.273
  3.0 6.4 %all-to-all-start.1 = ((bf16[16,2,32]{2,1,0:T(2,128)(2,1)}), bf16[16,2,32]{2,1,0:T(2,128)(2,1)S(1)}, u32[]{:S(2)}, u32[]{:S(2)}) async-start(bf16[16,2,32]{2,1,0:T(2,128)(2,1)} %reshape.273), calls=%async_computation.1 | async-start | bytes 16384 | tf_op jit(solution)/shard_map/all_to_all | solution.py:92
  9.4 0.7 add_convert_fusion.1
  10.1 0.7 iota_compare_fusion.1
  10.8 0.8 copy.46
  11.6 0.7 broadcast_multiply_fusion
  12.3 0.1 eq.15
  12.4 0.1 fusion.42
  12.5 0.2 select_reduce_fusion
  12.7 0.1 copy.45
  12.8 0.1 mul.205
  13.0 0.1 reshape.301
  13.1 6.4 %scatter_fusion = s32[4,64]{1,0:T(4,128)S(1)} fusion(s32[4,64]{1,0:T(4,128)S(1)} %broadcast.223, s32[128]{0:T(128)S(1)} %reshape.299, s32[128]{0:T(128)S(1)} %reshape.301), kind=kCustom, calls=%fused_computation.2 | custom fusion | bytes 2560 | tf_op jit(solution)/shard_map/vmap()/scatter | solution.py:38
  19.6 0.1 reshape.275
  19.7 0.1 reshape_transpose.3
  19.9 0.2 convolution_convert_fusion.5
  20.1 0.1 reshape.272
  20.3 0.1 copy.48
  20.4 0.1 reshape.307
  20.5 6.4 %scatter_fusion.1 = f32[4,64]{1,0:T(4,128)S(1)} fusion(f32[4,64]{1,0:T(4,128)S(1)} %broadcast_in_dim.26, s32[128]{0:T(128)S(1)} %reshape.299, f32[128]{0:T(128)S(1)} %reshape.307), kind=kCustom, calls=%fused_computation.3 | custom fusion | bytes 2560 | tf_op jit(solution)/shard_map/vmap()/scatter | solution.py:40
  27.0 0.1 multiply_cosine_fusion
  27.2 0.1 fusion.20
  27.3 0.6 copy.39
  28.0 5.1 %all-to-all-start = ((bf16[16,2,512]{2,1,0:T(2,128)(2,1)}), bf16[16,2,512]{2,1,0:T(2,128)(2,1)S(1)}, u32[]{:S(2)}, u32[]{:S(2)}) async-start(bf16[16,2,512]{2,1,0:T(2,128)(2,1)} %copy.39), calls=%async_computation | async-start | bytes 65536 | tf_op jit(solution)/shard_map/all_to_all | solution.py:91
  33.2 5.7 %all-to-all-done = bf16[16,2,512]{2,1,0:T(2,128)(2,1)S(1)} async-done(((bf16[16,2,512]{2,1,0:T(2,128)(2,1)}), bf16[16,2,512]{2,1,0:T(2,128)(2,1)S(1)}, u32[]{:S(2)}, u32[]{:S(2)}) %all-to-all-start) | async-done | bytes 32800 | tf_op jit(solution)/shard_map/all_to_all | solution.py:91
  38.9 5.7 %fusion.66 = f32[2,16,4096]{2,1,0:T(8,128)S(1)} fusion(bf16[2,16,512]{2,1,0:T(8,128)(2,1)S(1)} %all_to_all.36, bf16[2,4096,512]{2,1,0:T(8,128)(2,1)} %param.23), kind=kOutput, calls=%fused_computation.111 | convolution fusion | flops 134217728 | bytes 8945664 | tf_op jit(solution)/shard_map/bhc,bpc->bhp/dot_general | solution.py:96
  44.6 0.3 fusion.3
  44.9 0.3 fusion.65
  45.2 4.7 %convolution_convert_fusion.1 = bf16[2,16,512]{2,1,0:T(8,128)(2,1)S(1)} fusion(bf16[2,4096,512]{2,1,0:T(8,128)(2,1)} %param.23, f32[2,16]{1,0:T(2,128)S(1)} %fusion.65, f32[2,16,4096]{2,1,0:T(8,128)S(1)} %fusion.3), kind=kOutput, calls=%fused_computation.20 | convolution fusion | flops 134631456 | bytes 8945792 | tf_op jit(solution)/shard_map/bhp,bpc->bhc/dot_general | solution.py:110
  49.9 0.6 copy.42
  50.6 3.3 %all-to-all-start.2 = ((bf16[2,16,512]{2,0,1:T(2,128)(2,1)}), bf16[2,16,512]{2,0,1:T(2,128)(2,1)S(1)}, u32[]{:S(2)}, u32[]{:S(2)}) async-start(bf16[2,16,512]{2,0,1:T(2,128)(2,1)} %copy.42), calls=%async_computation.2 | async-start | bytes 65536 | tf_op jit(solution)/shard_map/all_to_all | solution.py:113
  53.9 5.7 %all-to-all-done.2 = bf16[2,16,512]{2,0,1:T(2,128)(2,1)S(1)} async-done(((bf16[2,16,512]{2,0,1:T(2,128)(2,1)}), bf16[2,16,512]{2,0,1:T(2,128)(2,1)S(1)}, u32[]{:S(2)}, u32[]{:S(2)}) %all-to-all-start.2) | async-done | bytes 32800 | tf_op jit(solution)/shard_map/all_to_all | solution.py:113
  59.6 0.1 fusion.21
  59.8 0.1 reshape.274
  59.9 0.2 convolution_convert_fusion
  60.1 15.1 %all-gather = bf16[128,2048]{1,0:T(8,128)(2,1)S(1)} all-gather(bf16[16,2048]{1,0:T(8,128)(2,1)S(1)} %convolution_convert_fusion), channel_id=2, replica_groups=mesh['ep'=4,'tp'=8] {'tp'}, dimensions={0}, use_global_device_ids=true | all-gather | bytes 589824 | tf_op jit(solution)/shard_map/all_gather | solution.py:7
  75.2 0.1 fusion.32
  75.3 0.2 fusion.34
  75.7 9.0 %all_gather.11 = bf16[64,2048]{1,0:T(8,128)(2,1)S(1)} all-gather(bf16[16,2048]{1,0:T(8,128)(2,1)S(1)} %fusion.36), channel_id=1, replica_groups=mesh['ep'=4,'tp'=8] {'ep'}, dimensions={0}, use_global_device_ids=true | all-gather | bytes 327680 | tf_op jit(solution)/shard_map/all_gather | solution.py:131
  84.7 0.7 gather_fusion
  85.4 2.7 %fusion.9 = f32[64,896]{1,0:T(8,128)S(1)} fusion(bf16[64,2048]{1,0:T(8,128)(2,1)S(1)} %gather_fusion, bf16[1,2048,896]{2,1,0:T(8,128)(2,1)} %param.32), kind=kOutput, calls=%fused_computation.14 | convolution fusion | flops 234881024 | bytes 4161536 | tf_op jit(solution)/shard_map/jnd,jdf->jnf/dot_general | solution.py:46
  88.2 4.7 %fusion.11 = f32[64,2048]{1,0:T(8,128)S(1)} fusion(bf16[1,896,2048]{2,1,0:T(8,128)(2,1)} %param.34, bf16[64,2048]{1,0:T(8,128)(2,1)S(1)} %gather_fusion, bf16[1,2048,896]{2,1,0:T(8,128)(2,1)} %param.33, f32[64]{0:T(128)S(1)} %mul.215, f32[64,896]{1,0:T(8,128)S(1)} %fusion.9), kind=kOutput, calls=%fused_computation.16 | convolution fusion | flops 470237184 | bytes 8356096 | tf_op jit(solution)/shard_map/jnf,jfd->jnd/dot_general | solution.py:49
  92.9 1.5 %scatter_custom_fusion = f32[65,2048]{1,0:T(8,128)S(1)} fusion(s32[64]{0:T(128)S(1)} %fusion.59, f32[64,2048]{1,0:T(8,128)S(1)} %fusion.11, f32[]{:T(128)} %constant.24.clone.1), kind=kCustom, calls=%fused_computation.28 | custom fusion | flops 131072 | bytes 532484 | tf_op jit(solution)/shard_map/scatter-add | solution.py:159
  94.5 43.9 %all-reduce.3 = bf16[64,2048]{1,0:T(8,128)(2,1)S(1)} all-reduce(f32[64,2048]{1,0:T(8,128)S(1)} %slice.20), channel_id=3, replica_groups=mesh['ep'=4,'tp'=8] {'ep','tp'}, use_global_device_ids=true, to_apply=%region_13.14.clone | all-reduce | flops 131072 | bytes 786432
  138.4 0.1 fusion.43
  138.5 0.7 fusion.46
  (59 shorter events, 1.1 us)
Async XLA Ops:
  0.0 44.6 %copy-start = (bf16[2,32,4096]{2,1,0:T(8,128)(2,1)S(1)}, bf16[2,32,4096]{2,1,0:T(8,128)(2,1)}, u32[]{:S(2)}) copy-start(bf16[2,32,4096]{2,1,0:T(8,128)(2,1)} %param.24) | copy-start | bytes 1572868
  0.0 19.9 %copy-start.1 = (bf16[16,2048]{1,0:T(8,128)(2,1)S(1)}, bf16[16,2048]{1,0:T(8,128)(2,1)}, u32[]{:S(2)}) copy-start(bf16[16,2048]{1,0:T(8,128)(2,1)} %param.18) | copy-start | bytes 196612
  0.0 19.9 %copy-start.7 = (f32[2048]{0:T(1024)S(1)}, f32[2048]{0:T(1024)}, u32[]{:S(2)}) copy-start(f32[2048]{0:T(1024)} %param.19) | copy-start | bytes 24580
  0.0 19.9 %copy-start.3 = (bf16[2048,128]{1,0:T(8,128)(2,1)S(1)}, bf16[2048,128]{1,0:T(8,128)(2,1)}, u32[]{:S(2)}) copy-start(bf16[2048,128]{1,0:T(8,128)(2,1)} %param.20) | copy-start | bytes 1572868
  0.0 20.2 %copy-start.6 = (f32[64,2]{0,1:T(2,128)S(1)}, f32[64,2]{0,1:T(2,128)}, u32[]{:S(2)}) copy-start(f32[64,2]{0,1:T(2,128)} %param.31) | copy-start | bytes 1540
  3.0 25.0 %all-to-all-start.1 = ((bf16[16,2,32]{2,1,0:T(2,128)(2,1)}), bf16[16,2,32]{2,1,0:T(2,128)(2,1)S(1)}, u32[]{:S(2)}, u32[]{:S(2)}) async-start(bf16[16,2,32]{2,1,0:T(2,128)(2,1)} %reshape.273), calls=%async_computation.1 | async-start | bytes 16384 | tf_op jit(solution)/shard_map/all_to_all | solution.py:92
  13.1 14.0 %copy-start.4 = (bf16[2,64,512]{2,1,0:T(8,128)(2,1)S(1)}, bf16[2,64,512]{2,1,0:T(8,128)(2,1)}, u32[]{:S(2)}) copy-start(bf16[2,64,512]{2,1,0:T(8,128)(2,1)} %param.22) | copy-start | bytes 393220
  28.0 10.8 %all-to-all-start = ((bf16[16,2,512]{2,1,0:T(2,128)(2,1)}), bf16[16,2,512]{2,1,0:T(2,128)(2,1)S(1)}, u32[]{:S(2)}, u32[]{:S(2)}) async-start(bf16[16,2,512]{2,1,0:T(2,128)(2,1)} %copy.39), calls=%async_computation | async-start | bytes 65536 | tf_op jit(solution)/shard_map/all_to_all | solution.py:91
  45.1 14.5 %copy-start.5 = (bf16[2,512,64]{1,2,0:T(8,128)(2,1)S(1)}, bf16[2,512,64]{1,2,0:T(8,128)(2,1)}, u32[]{:S(2)}) copy-start(bf16[2,512,64]{1,2,0:T(8,128)(2,1)} %param.26) | copy-start | bytes 393220
  45.1 14.7 %copy-start.2 = (bf16[128,2048]{1,0:T(8,128)(2,1)S(1)}, bf16[128,2048]{1,0:T(8,128)(2,1)}, u32[]{:S(2)}) copy-start(bf16[128,2048]{1,0:T(8,128)(2,1)} %param.27) | copy-start | bytes 1572868
  45.2 30.2 %copy-start.8 = (f32[2048]{0:T(1024)S(1)}, f32[2048]{0:T(1024)}, u32[]{:S(2)}) copy-start(f32[2048]{0:T(1024)} %param.28) | copy-start | bytes 24580
  45.2 30.4 %copy-start.9 = (f32[2048]{0:T(1024)S(1)}, f32[2048]{0:T(1024)}, u32[]{:S(2)}) copy-start(f32[2048]{0:T(1024)} %param.29) | copy-start | bytes 24580
  50.6 9.0 %all-to-all-start.2 = ((bf16[2,16,512]{2,0,1:T(2,128)(2,1)}), bf16[2,16,512]{2,0,1:T(2,128)(2,1)S(1)}, u32[]{:S(2)}, u32[]{:S(2)}) async-start(bf16[2,16,512]{2,0,1:T(2,128)(2,1)} %copy.42), calls=%async_computation.2 | async-start | bytes 65536 | tf_op jit(solution)/shard_map/all_to_all | solution.py:113
  88.2 50.3 %copy-start.10 = (f32[2048]{0:T(1024)S(1)}, f32[2048]{0:T(1024)}, u32[]{:S(2)}) copy-start(f32[2048]{0:T(1024)} %param.35) | copy-start | bytes 24580
